TPU v7x, 32 devices: a whole 2x2x4 slice. The times are simulated.
32 devices in a mesh: sp: 8 (over z, x), tp: 4 (over y, core).
Axes of the slice: x: 2, y: 2, z: 4, core: 2. Of those that a mesh axis runs over, the one named last changes fastest.
Arguments:
- tokens: bfloat16 [4096, 2048], P(('sp', 'tp')), may hold values from -6 to 6
- norm_gain: float32 [2048], replicated, may hold values from 0.1 to 1.9
- w_query: bfloat16 [2048, 1024], P(None, 'tp'), may hold values from -16 to 16
- w_key: bfloat16 [2048, 1024], P(None, 'tp'), may hold values from -16 to 16
- w_value: bfloat16 [2048, 1024], P(None, 'tp'), may hold values from -0.125 to 0.125
- conv_in: bfloat16 [2048, 2048], P(None, 'tp'), may hold values from -0.125 to 0.125
- conv_gate: bfloat16 [2048, 2048], P(None, 'tp'), may hold values from -0.125 to 0.125
- conv_taps: float32 [31, 2048], P(None, 'tp'), may hold values from -3.7 to 3.7
- conv_gain: float32 [2048], P('tp'), may hold values from 0.1 to 1.9
- cum_gate: float32 [16, 4096], P('tp'), may hold values from -514 to 0, as said below
- out_attn: bfloat16 [1024, 2048], P('tp'), may hold values from -0.75 to 0.75
- out_conv: bfloat16 [2048, 2048], P('tp'), may hold values from -0.125 to 0.125
Outputs:
- mixed: bfloat16 [4096, 2048], P(('sp', 'tp'))
- log_total: float32 [16, 4096], P('tp', 'sp')
Inputs may be any that keep to these rules, and one draw needn't show every extreme that they name: `cum_gate`: for each head the values never rise from one position to the next and are at most 0.
All inputs are finite; a program needn't handle non-finite values.
Results may differ from a plain program's by a relative error of at most 0.014.
Values may be sent and summed in bfloat16 or wider, within the bound.
A program may use at most 128 MiB of HBM per device.

v0:
```python
import jax
import jax.numpy as jnp
from jax import lax
from jax.sharding import PartitionSpec as P

HEAD = 64


def shifted(array, axis, by):
    length = lax.axis_size(axis)
    pairs = [(i, i + by) for i in range(length) if 0 <= i + by < length]
    return lax.ppermute(array, axis, pairs)


def per_device(
    tokens,
    norm_gain,
    w_query,
    w_key,
    w_value,
    conv_in,
    conv_gate,
    conv_taps,
    conv_gain,
    cum_gate,
    out_attn,
    out_conv,
):
    heads_here = w_query.shape[1] // HEAD
    width_att = w_query.shape[1]
    channels = conv_in.shape[1]
    kernel_len = conv_taps.shape[0]
    wide = lax.all_gather(tokens, "tp", axis=0, tiled=True).astype(jnp.float32)
    factor = lax.rsqrt(jnp.mean(wide * wide, axis=1, keepdims=True) + 1e-06)
    normed = (wide * factor * norm_gain[None, :]).astype(jnp.bfloat16)
    query = (jnp.dot(normed, w_query, preferred_element_type=jnp.float32) * HEAD ** (-0.5)).astype(
        jnp.bfloat16
    )
    keyed = jnp.dot(normed, w_key, preferred_element_type=jnp.float32).astype(jnp.bfloat16)
    valued = jnp.dot(normed, w_value, preferred_element_type=jnp.float32).astype(jnp.bfloat16)
    opened = jnp.dot(normed, conv_in, preferred_element_type=jnp.float32)
    gating = jnp.dot(normed, conv_gate, preferred_element_type=jnp.float32)
    gated_rows = (opened * jax.nn.sigmoid(gating)).astype(jnp.bfloat16)
    joined = jnp.concatenate([query, keyed, valued, gated_rows], axis=1)
    local_rows = joined.shape[0]
    own_index = lax.axis_index("sp")
    offset = own_index * local_rows
    query_rows = joined[:, :width_att]
    key_rows = joined[:, width_att : 2 * width_att]
    value_rows = joined[:, 2 * width_att : 3 * width_att]
    gated = joined[:, 3 * width_att :]
    group_list = (query_rows, offset)
    group_data = []
    group_rows, group_start = group_list
    count_rows = group_rows.shape[0]
    group_data.append(
        (
            group_rows.reshape(count_rows, heads_here, HEAD),
            lax.dynamic_slice_in_dim(cum_gate, group_start, count_rows, 1),
            group_start + jnp.arange(count_rows, dtype=jnp.int32),
            group_start + count_rows - 1,
        )
    )

    def absorb(carry_in, group, key_block, value_block, first_place):
        query_heads, cum_query, query_place, last_query = group
        row_best, row_total, row_accum = carry_in
        length_in = key_block.shape[0]
        key_heads = key_block.reshape(length_in, heads_here, HEAD)
        value_heads = value_block.reshape(length_in, heads_here, HEAD)
        cum_keys = lax.dynamic_slice_in_dim(cum_gate, first_place, length_in, 1)
        scores = jnp.einsum(
            "qhd,khd->hqk", query_heads, key_heads, preferred_element_type=jnp.float32
        )
        scores = scores + cum_query[:, :, None] - cum_keys[:, None, :]
        key_place = first_place + jnp.arange(length_in, dtype=jnp.int32)
        visible = jnp.logical_and(
            key_place[None, :] <= query_place[:, None], key_place[None, :] >= 0
        )[None]
        scores = jnp.where(visible, scores, -1e30)
        new_best = jnp.maximum(row_best, jnp.max(scores, axis=2))
        shrink = jnp.exp(row_best - new_best)
        weights = jnp.where(visible, jnp.exp(scores - new_best[:, :, None]), 0.0)
        row_total = shrink * row_total + jnp.sum(weights, axis=2)
        row_accum = shrink[:, :, None] * row_accum + jnp.einsum(
            "hqk,khd->hqd",
            weights.astype(jnp.bfloat16),
            value_heads,
            preferred_element_type=jnp.float32,
        )
        return (new_best, row_total, row_accum)

    initial = tuple(
        (
            (
                jnp.full((heads_here, group[0].shape[0]), -1e30, jnp.float32),
                jnp.zeros((heads_here, group[0].shape[0]), jnp.float32),
                jnp.zeros((heads_here, group[0].shape[0], HEAD), jnp.float32),
            )
            for group in group_data
        )
    )
    key_group = lax.all_gather(key_rows, "sp", axis=0, tiled=True)
    value_group = lax.all_gather(value_rows, "sp", axis=0, tiled=True)
    length_in = key_group.shape[0]
    turns = length_in // local_rows

    def advance(turn_index, carry_now):
        begin_row = turn_index * local_rows
        key_block = lax.dynamic_slice_in_dim(key_group, begin_row, local_rows, 0)
        value_block = lax.dynamic_slice_in_dim(value_group, begin_row, local_rows, 0)
        updated = []
        for group, inner_carry in zip(group_data, carry_now):
            wanted = jnp.logical_and(begin_row <= group[3], begin_row + local_rows > 0)

            def take_block(inner, group=group):
                return absorb(inner, group, key_block, value_block, begin_row)

            def skip_block(inner):
                return inner

            updated.append(lax.cond(wanted, take_block, skip_block, inner_carry))
        return tuple(updated)

    carry = lax.fori_loop(0, turns, advance, initial)
    attended_parts = []
    total_parts = []
    for row_best, row_total, row_accum in carry:
        count_rows = row_total.shape[1]
        attended_parts.append(
            (row_accum / row_total[:, :, None])
            .astype(jnp.bfloat16)
            .transpose(1, 0, 2)
            .reshape(count_rows, width_att)
        )
        total_parts.append(row_best + jnp.log(row_total))
    attended = attended_parts[0]
    log_total = total_parts[0]
    rim_rows = shifted(gated[local_rows - (kernel_len - 1) :], "sp", 1)
    padded = jnp.concatenate([rim_rows, gated], axis=0).astype(jnp.float32)
    convolved = jnp.zeros((local_rows, channels), jnp.float32)
    for tap_index in range(kernel_len):
        convolved = (
            convolved + conv_taps[tap_index][None, :] * padded[tap_index : tap_index + local_rows]
        )
    all_channels = channels * lax.axis_size("tp")
    channel_square = lax.psum(jnp.sum(convolved * convolved, axis=1), "tp") / all_channels
    conv_out = jax.nn.silu(
        convolved * lax.rsqrt(channel_square + 1e-06)[:, None] * conv_gain[None, :]
    ).astype(jnp.bfloat16)
    group_part = jnp.dot(attended, out_attn, preferred_element_type=jnp.float32)
    group_part = group_part + jnp.dot(conv_out, out_conv, preferred_element_type=jnp.float32)
    mixed = lax.psum_scatter(
        lax.optimization_barrier(group_part.astype(jnp.bfloat16))
        .astype(jnp.float32)
        .astype(jnp.bfloat16),
        "tp",
        scatter_dimension=0,
        tiled=True,
    )
    return (mixed, log_total)


def solution(mesh):
    in_specs = (
        P(("sp", "tp"), None),
        P(),
        P(None, "tp"),
        P(None, "tp"),
        P(None, "tp"),
        P(None, "tp"),
        P(None, "tp"),
        P(None, "tp"),
        P("tp"),
        P("tp", None),
        P("tp", None),
        P("tp", None),
    )
    out_specs = (P(("sp", "tp"), None), P("tp", "sp"))
    return jax.shard_map(
        per_device, mesh=mesh, in_specs=in_specs, out_specs=out_specs, check_vma=False
    )
```

profile of v0, /device:TPU:0, one launch (start us, length us, event | category | flops | bytes accessed | tf_op | source)
XLA Modules:
  0.0 236.0 jit_solution(1296425185891095124)
XLA Ops:
  8.0 26.9 %all-gather.4.cloned.1.call-done = bf16[512,2048]{1,0:T(8,128)(2,1)} async-done(((bf16[128,2048]{1,0:T(8,128)(2,1)}), bf16[512,2048]{1,0:T(8,128)(2,1)}) %all-gather.4.cloned.1.call-update) | async-done | bytes 2097168 | tf_op jit(solution)/shard_map/all_gather | solution.py:33
  34.9 2.1 fusion.13
  37.0 3.3 %convolution_convert_fusion.1 = bf16[512,256]{1,0:T(8,128)(2,1)} fusion(bf16[2048,256]{1,0:T(8,128)(2,1)} %param.19, bf16[512,2048]{1,0:T(8,128)(2,1)} %all-gather.4.cloned.1.call-done, f32[2048]{0:T(1024)} %param.17, f32[512]{0:T(512)S(1)} %add_rsqrt_fusion.1), kind=kOutput, calls=%fused_computation.35 | convolution fusion | flops 541196288 | bytes 3418112 | tf_op jit(solution)/shard_map/dot_general | solution.py:39
  40.4 3.0 %convolution_convert_fusion = bf16[512,256]{1,0:T(8,128)(2,1)} fusion(bf16[2048,256]{1,0:T(8,128)(2,1)S(1)} %copy-done.5, bf16[512,2048]{1,0:T(8,128)(2,1)} %all-gather.4.cloned.1.call-done, f32[2048]{0:T(1024)S(1)} %copy-done.7, f32[512]{0:T(512)S(1)} %add_rsqrt_fusion.1), kind=kOutput, calls=%fused_computation.34 | convolution fusion | flops 541196288 | bytes 3418112 | tf_op jit(solution)/shard_map/dot_general | solution.py:40
  44.3 3.8 %fusion.18 = f32[512,512]{1,0:T(8,128)S(1)} fusion(bf16[2048,512]{1,0:T(8,128)(2,1)} %param.22, bf16[512,2048]{1,0:T(8,128)(2,1)} %all-gather.4.cloned.1.call-done, f32[2048]{0:T(1024)S(1)} %copy-done.7, f32[512]{0:T(512)S(1)} %add_rsqrt_fusion.1), kind=kOutput, calls=%fused_computation.30 | convolution fusion | flops 1078722560 | bytes 5253120 | tf_op jit(solution)/shard_map/dot_general | solution.py:42
  48.2 1.3 fusion.19
  49.5 3.4 %collective-permute-start = (bf16[30,512]{1,0:T(8,128)(2,1)S(1)}, bf16[30,512]{1,0:T(8,128)(2,1)S(1)}, u32[]{:S(2)}, u32[]{:S(2)}) collective-permute-start(bf16[30,512]{1,0:T(8,128)(2,1)S(1)} %slice.252), channel_id=1, source_target_pairs={{0,4},{4,8},{8,12},{12,16},{16,20},{20,24},{24,28},{1,5},{5,9},{9,... | collective-permute-start | bytes 92168 | tf_op jit(solution)/shard_map/ppermute | solution.py:12
  52.9 1.0 fusion.20
  54.6 5.7 %multiply_reduce_fusion = (f32[512]{0:T(512)S(1)}, f32[512,512]{1,0:T(8,128)}) fusion(f32[542,512]{1,0:T(8,128)S(1)} %maximum_convert_fusion, f32[512]{0:T(512)S(1)} %bitcast.72, f32[512]{0:T(512)S(1)} %bitcast.73, f32[512]{0:T(512)S(1)} %bitcast.75, f32[512]{0:T(512)S(1)} %bitcast.76, f32[512]{0:T(512)S(1)} %bitcast.77, f32[512]{0:T(512)S(1)} %bitcast.78, ...), kind=kLoop, calls=%fused_computation.98 | loop fusion | flops 16514560 | bytes 33619968 | tf_op jit(solution)/shard_map/reduce_sum | solution.py:147
  60.3 6.1 %psum.7 = f32[512]{0:T(512)S(1)} all-reduce(f32[512]{0:T(512)S(1)} %get-tuple-element.390), channel_id=1, replica_groups=mesh['sp'=8,'tp'=4] {'tp'}, use_global_device_ids=true, to_apply=%region_8.9 | all-reduce | flops 512 | bytes 4096 | tf_op jit(solution)/shard_map/psum | solution.py:147
  66.4 23.3 %all-gather.6.cloned.1.call-done = bf16[4096,256]{1,0:T(8,128)(2,1)} async-done(((bf16[512,256]{1,0:T(8,128)(2,1)}), bf16[4096,256]{1,0:T(8,128)(2,1)}) %all-gather.6.cloned.1.call-update) | async-done | bytes 2097168 | tf_op jit(solution)/shard_map/all_gather | solution.py:103
  89.7 4.1 %copy.15 = bf16[4096,256]{0,1:T(8,128)(2,1)} copy(bf16[4096,256]{1,0:T(8,128)(2,1)} %all-gather.6.cloned.1.call-done) | data formatting | bytes 4194304
  93.8 45.7 %all-gather.8.cloned.1.call-done = bf16[4096,256]{1,0:T(8,128)(2,1)} async-done(((bf16[512,256]{1,0:T(8,128)(2,1)}), bf16[4096,256]{1,0:T(8,128)(2,1)}) %all-gather.8.cloned.1.call-update) | async-done | bytes 2097168 | tf_op jit(solution)/shard_map/all_gather | solution.py:104
  139.5 4.1 %copy.16 = bf16[4096,256]{0,1:T(8,128)(2,1)} copy(bf16[4096,256]{1,0:T(8,128)(2,1)} %all-gather.8.cloned.1.call-done) | data formatting | bytes 4194304
  143.7 6.8 %while.18 = (s32[]{:T(128)}, f32[4,512]{1,0:T(4,128)S(1)}, f32[4,512]{1,0:T(4,128)S(1)}, f32[4,512,64]{1,2,0:T(8,128)S(1)}, s32[]{:T(128)}, /*index=5*/bf16[4096...) while((s32[]{:T(128)}, f32[4,512]{1,0:T(4,128)S(1)}, ...), condition=%wide.region_6.7_spmd.clone, body=%wide.region_1.6_spmd.clone.sunk | while | flops 286005248 | bytes 16725373 | solution.py:125
  143.8 6.3 %conditional.3 = ((f32[4,512]{1,0:T(4,128)S(1)}, f32[4,512]{1,0:T(4,128)S(1)}, f32[4,512,64]{1,2,0:T(8,128)S(1)})) conditional(s32[]{:T(128)} %convert_element_type.89, (f32[4,512]{1,0:T(4,128)S(1)}, f32[4,512]{1,0:T(4,128)S(1)}, f32[4,512,64]{1,2,0:T(8,128)S(1)}) %tuple.88, (s32[]{:T(128)}, s32[]{:T(128)}, bf16[4096,256]{0,1:T(8,128)(2,1)}, ...), branch_computations={%region_2.0_spmd, %region_3.5_spmd} | conditional | flops 286005248 | bytes 16723030 | solution.py:122
  144.1 0.7 constant_dynamic-slice_fusion.1
  144.8 1.1 constant_dynamic-slice_fusion
  145.8 1.2 fusion.4
  147.0 1.4 fusion.3
  148.4 1.6 fusion.8
  150.6 2.0 fusion.63
  152.7 2.8 %add_convert_fusion = bf16[512,2048]{1,0:T(8,128)(2,1)} fusion(f32[512,2048]{1,0:T(8,128)S(1)} %fusion.63, bf16[512,2048]{1,0:T(8,128)(2,1)S(1)} %copy-done, f32[512,512]{1,0:T(8,128)S(1)} %copy-done.2, f32[512]{0:T(512)S(1)} %copy-done.8, f32[512]{0:T(512)S(1)} %add_rsqrt_fusion), kind=kOutput, calls=%fused_computation.25 | convolution fusion | flops 1077673984 | bytes 9441280 | tf_op jit(solution)/shard_map/dot_general | solution.py:152
  156.1 73.3 %reduce-scatter.2.cloned.1.call-done = bf16[128,2048]{1,0:T(8,128)(2,1)} async-done(((bf16[512,2048]{1,0:T(8,128)(2,1)}), bf16[128,2048]{1,0:T(8,128)(2,1)}) %reduce-scatter.2.cloned.1.call-update) | async-done | bytes 524304 | tf_op jit(solution)/shard_map/reduce_scatter | solution.py:153
  (60 shorter events, 3.6 us)
Async XLA Ops:
  7.2 145.5 %copy-start = (bf16[512,2048]{1,0:T(8,128)(2,1)S(1)}, bf16[512,2048]{1,0:T(8,128)(2,1)}, u32[]{:S(2)}) copy-start(bf16[512,2048]{1,0:T(8,128)(2,1)} %param.27) | copy-start | bytes 6291460
  7.2 27.7 %all-gather.4.cloned.1.call-start = ((), (), s32[]{:S(2)}) async-start(), calls=%async_computation.1 | async-start | bytes 2621440 | tf_op jit(solution)/shard_map/all_gather | solution.py:33
  7.9 32.5 %copy-start.5 = (bf16[2048,256]{1,0:T(8,128)(2,1)S(1)}, bf16[2048,256]{1,0:T(8,128)(2,1)}, u32[]{:S(2)}) copy-start(bf16[2048,256]{1,0:T(8,128)(2,1)} %param.20) | copy-start | bytes 3145732
  7.9 32.5 %copy-start.7 = (f32[2048]{0:T(1024)S(1)}, f32[2048]{0:T(1024)}, u32[]{:S(2)}) copy-start(f32[2048]{0:T(1024)} %param.17) | copy-start | bytes 24580
  7.9 81.8 %all-gather.6.cloned.1.call-start = ((), (), s32[]{:S(2)}) async-start(), calls=%async_computation.2 | async-start | bytes 2359296 | tf_op jit(solution)/shard_map/all_gather | solution.py:103
  40.3 3.9 %copy-start.3 = (f32[31,512]{1,0:T(8,128)S(1)}, f32[31,512]{1,0:T(8,128)}, u32[]{:S(2)}) copy-start(f32[31,512]{1,0:T(8,128)} %param.23) | copy-start | bytes 190468
  40.3 99.2 %all-gather.8.cloned.1.call-start = ((), (), s32[]{:S(2)}) async-start(), calls=%async_computation.3 | async-start | bytes 2359296 | tf_op jit(solution)/shard_map/all_gather | solution.py:104
  43.5 186.0 %reduce-scatter.2.cloned.1.call-start = ((), (), s32[]{:S(2)}) async-start(), calls=%async_computation.4 | async-start | bytes 2621440 | tf_op jit(solution)/shard_map/reduce_scatter | solution.py:153
  44.3 3.8 %copy-start.1 = (bf16[512,2048]{1,0:T(8,128)(2,1)S(1)}, bf16[512,2048]{1,0:T(8,128)(2,1)}, u32[]{:S(2)}) copy-start(bf16[512,2048]{1,0:T(8,128)(2,1)} %all-gather.4.cloned.1.call-done) | copy-start | bytes 6291460
  44.3 3.8 %copy-start.4 = (bf16[2048,512]{1,0:T(8,128)(2,1)S(1)}, bf16[2048,512]{1,0:T(8,128)(2,1)}, u32[]{:S(2)}) copy-start(bf16[2048,512]{1,0:T(8,128)(2,1)} %param.21) | copy-start | bytes 6291460
  48.1 4.7 %copy-start.6 = (bf16[2048,256]{1,0:T(8,128)(2,1)S(1)}, bf16[2048,256]{1,0:T(8,128)(2,1)}, u32[]{:S(2)}) copy-start(bf16[2048,256]{1,0:T(8,128)(2,1)} %param.18) | copy-start | bytes 3145732
  49.5 5.0 %collective-permute-start = (bf16[30,512]{1,0:T(8,128)(2,1)S(1)}, bf16[30,512]{1,0:T(8,128)(2,1)S(1)}, u32[]{:S(2)}, u32[]{:S(2)}) collective-permute-start(bf16[30,512]{1,0:T(8,128)(2,1)S(1)} %slice.252), channel_id=1, source_target_pairs={{0,4},{4,8},{8,12},{12,16},{16,20},{20,24},{24,28},{1,5},{5,9},{9,... | collective-permute-start | bytes 92168 | tf_op jit(solution)/shard_map/ppermute | solution.py:12
  150.5 2.1 copy-start.2
  150.5 2.1 copy-start.8
Sparse Core Ops, SparseCore 0:
  9.5 25.2 all-gather.3
  40.4 49.2 all-gather.5
  91.9 47.6 all-gather.7
  155.6 73.7 reduce-scatter.1
where the time goes:
time: 237 us; the launch traced here: 236 us
  waiting for transfers between devices  171 us (72%)
  matrix products  20.1 us (8%)
  between operations  14 us (6%)
  local copies, waits for them, and re-layouts  10.9 us (5%)
  other arithmetic  10.3 us (4%)
  blocking collectives  6.08 us (3%)
  starting transfers between devices  3.54 us (1%)
    reduce_scatter x1, waiting for transfers between devices, per_device(): lax.psum_scatter(lax.optimization_barrier(group_part.astype(jnp.bfloat16)...  73.3 us
    all_gather x1, waiting for transfers between devices, per_device(): value_group = lax.all_gather(value_rows, 'sp', axis=0, tiled=True)  45.7 us
    all_gather x1, waiting for transfers between devices, per_device(): wide = lax.all_gather(tokens, 'tp', axis=0, tiled=True).astype(jnp.float32)  26.9 us
    all_gather x1, waiting for transfers between devices, per_device(): key_group = lax.all_gather(key_rows, 'sp', axis=0, tiled=True)  23.3 us
    unnamed x20, local copies, waits for them, and re-layouts  8.28 us
    psum x1, blocking collectives, per_device(): lax.psum(jnp.sum(convolved * convolved, axis=1), 'tp') / all_channels  6.08 us
    reduce_sum x1, other arithmetic, per_device(): jnp.sum(convolved * convolved, axis=1)  5.69 us
  transfers between devices with their start and end apart: 5, of which 5 were waited for; matrix products, arithmetic and copies ran while one was open for 9% of the time, Pallas kernels for 0%

commit v1 on v0

--- a/solution.py
+++ b/solution.py
@@ -30,7 +30,9 @@
     width_att = w_query.shape[1]
     channels = conv_in.shape[1]
     kernel_len = conv_taps.shape[0]
-    wide = lax.all_gather(tokens, "tp", axis=0, tiled=True).astype(jnp.float32)
+    wide = jnp.concatenate(
+        lax.all_to_all(jnp.stack([tokens] * lax.axis_size("tp")), "tp", 0, 0), axis=0
+    ).astype(jnp.float32)
     factor = lax.rsqrt(jnp.mean(wide * wide, axis=1, keepdims=True) + 1e-06)
     normed = (wide * factor * norm_gain[None, :]).astype(jnp.bfloat16)
     query = (jnp.dot(normed, w_query, preferred_element_type=jnp.float32) * HEAD ** (-0.5)).astype(

time: 237 us -> 239 us (level)
  blocking collectives: 6.08 us -> 35.7 us
  waiting for transfers between devices: 171 us -> 144 us
  local copies, waits for them, and re-layouts: 10.9 us -> 13.9 us
    all_to_all x0 -> x1, blocking collectives: none -> 29.7 us  [per_device(): lax.all_to_all(jnp.stack([tokens] * lax.axis_size('tp')), 'tp', 0, 0)]
    all_gather x1 -> x0, waiting for transfers between devices: 26.9 us -> none  [per_device(): wide = lax.all_gather(tokens, 'tp', axis=0, tiled=True).astype(jnp.float32)]
    unnamed x20 -> x24, local copies, waits for them, and re-layouts: 8.28 us -> 9.83 us
  transfers between devices with their start and end apart: 5 -> 4, of which waited for: 5 -> 4; matrix products, arithmetic and copies ran while one was open for 9% -> 8% of each run, Pallas kernels for 0% -> 0%
where the time goes in v1:
time: 239 us; the launch traced here: 238 us
  waiting for transfers between devices  144 us (60%)
  blocking collectives  35.7 us (15%)
  matrix products  17.9 us (7%)
  between operations  14 us (6%)
  local copies, waits for them, and re-layouts  13.9 us (6%)
  other arithmetic  9.23 us (4%)
  starting transfers between devices  3.52 us (1%)
    reduce_scatter x1, waiting for transfers between devices, per_device(): lax.psum_scatter(lax.optimization_barrier(group_part.astype(jnp.bfloat16)...  73.3 us
    all_gather x1, waiting for transfers between devices, per_device(): value_group = lax.all_gather(value_rows, 'sp', axis=0, tiled=True)  45.7 us
    all_to_all x1, blocking collectives, per_device(): lax.all_to_all(jnp.stack([tokens] * lax.axis_size('tp')), 'tp', 0, 0)  29.7 us
    all_gather x1, waiting for transfers between devices, per_device(): key_group = lax.all_gather(key_rows, 'sp', axis=0, tiled=True)  23.9 us
    unnamed x24, local copies, waits for them, and re-layouts  9.83 us
    psum x1, blocking collectives, per_device(): lax.psum(jnp.sum(convolved * convolved, axis=1), 'tp') / all_channels  5.92 us
    reduce_sum x1, other arithmetic, per_device(): jnp.sum(convolved * convolved, axis=1)  5.69 us
  transfers between devices with their start and end apart: 4, of which 4 were waited for; matrix products, arithmetic and copies ran while one was open for 8% of the time, Pallas kernels for 0%

profile of v1, /device:TPU:0, one launch (start us, length us, event | category | flops | bytes accessed | tf_op | source)
XLA Modules:
  0.0 238.4 jit_solution(16830933884112938600)
XLA Ops:
  7.2 1.4 stack.2
  8.7 29.7 %all_to_all.5 = bf16[4,128,2048]{2,1,0:T(8,128)(2,1)S(1)} all-to-all(bf16[4,128,2048]{2,1,0:T(8,128)(2,1)S(1)} %stack.2), channel_id=1, replica_groups=mesh['sp'=8,'tp'=4] {'tp'}, dimensions={0} | all-to-all | bytes 4194304 | tf_op jit(solution)/shard_map/all_to_all | solution.py:34
  39.6 1.3 copy-done.1
  41.0 1.4 convolution_convert_fusion.1
  42.5 3.0 %convolution_convert_fusion = bf16[512,256]{1,0:T(8,128)(2,1)} fusion(bf16[512,2048]{1,0:T(8,128)(2,1)} %copy-done.1, bf16[2048,256]{1,0:T(8,128)(2,1)S(1)} %copy-done.8), kind=kOutput, calls=%fused_computation.33 | convolution fusion | flops 537001984 | bytes 3407872 | tf_op jit(solution)/shard_map/dot_general | solution.py:42
  46.4 3.8 %fusion.17 = f32[512,512]{1,0:T(8,128)S(1)} fusion(bf16[512,2048]{1,0:T(8,128)(2,1)} %copy-done.1, bf16[2048,512]{1,0:T(8,128)(2,1)} %param.22), kind=kOutput, calls=%fused_computation.29 | convolution fusion | flops 1074528256 | bytes 5242880 | tf_op jit(solution)/shard_map/dot_general | solution.py:44
  50.2 1.3 fusion.18
  51.4 3.4 %collective-permute-start = (bf16[30,512]{1,0:T(8,128)(2,1)S(1)}, bf16[30,512]{1,0:T(8,128)(2,1)S(1)}, u32[]{:S(2)}, u32[]{:S(2)}) collective-permute-start(bf16[30,512]{1,0:T(8,128)(2,1)S(1)} %slice.252), channel_id=1, source_target_pairs={{0,4},{4,8},{8,12},{12,16},{16,20},{20,24},{24,28},{1,5},{5,9},{9,... | collective-permute-start | bytes 92168 | tf_op jit(solution)/shard_map/ppermute | solution.py:12
  55.6 0.8 collective-permute-done
  56.6 5.7 %multiply_reduce_fusion.1 = (f32[512]{0:T(512)S(1)}, f32[512,512]{1,0:T(8,128)}) fusion(f32[542,512]{1,0:T(8,128)S(1)} %maximum_convert_fusion, f32[512]{0:T(512)S(1)} %bitcast.85, f32[512]{0:T(512)S(1)} %bitcast.86, f32[512]{0:T(512)S(1)} %bitcast.88, f32[512]{0:T(512)S(1)} %bitcast.89, f32[512]{0:T(512)S(1)} %bitcast.90, f32[512]{0:T(512)S(1)} %bitcast.91, ...), kind=kLoop, calls=%fused_computation.97 | loop fusion | flops 16514560 | bytes 33619968 | tf_op jit(solution)/shard_map/reduce_sum | solution.py:149
  62.3 5.9 %psum.7 = f32[512]{0:T(512)S(1)} all-reduce(f32[512]{0:T(512)S(1)} %get-tuple-element.401), channel_id=1, replica_groups=mesh['sp'=8,'tp'=4] {'tp'}, use_global_device_ids=true, to_apply=%region_8.9 | all-reduce | flops 512 | bytes 4096 | tf_op jit(solution)/shard_map/psum | solution.py:149
  68.2 23.9 %all-gather.3.cloned.1.call-done = bf16[4096,256]{1,0:T(8,128)(2,1)} async-done(((bf16[512,256]{1,0:T(8,128)(2,1)}), bf16[4096,256]{1,0:T(8,128)(2,1)}) %all-gather.3.cloned.1.call-update) | async-done | bytes 2097168 | tf_op jit(solution)/shard_map/all_gather | solution.py:105
  92.1 4.1 %copy.18 = bf16[4096,256]{0,1:T(8,128)(2,1)} copy(bf16[4096,256]{1,0:T(8,128)(2,1)} %all-gather.3.cloned.1.call-done) | data formatting | bytes 4194304
  96.2 45.7 %all-gather.5.cloned.1.call-done = bf16[4096,256]{1,0:T(8,128)(2,1)} async-done(((bf16[512,256]{1,0:T(8,128)(2,1)}), bf16[4096,256]{1,0:T(8,128)(2,1)}) %all-gather.5.cloned.1.call-update) | async-done | bytes 2097168 | tf_op jit(solution)/shard_map/all_gather | solution.py:106
  141.9 4.1 %copy.19 = bf16[4096,256]{0,1:T(8,128)(2,1)} copy(bf16[4096,256]{1,0:T(8,128)(2,1)} %all-gather.5.cloned.1.call-done) | data formatting | bytes 4194304
  146.1 6.8 %while.18 = (s32[]{:T(128)}, f32[4,512]{1,0:T(4,128)S(1)}, f32[4,512]{1,0:T(4,128)S(1)}, f32[4,512,64]{1,2,0:T(8,128)S(1)}, s32[]{:T(128)}, /*index=5*/bf16[4096...) while((s32[]{:T(128)}, f32[4,512]{1,0:T(4,128)S(1)}, ...), condition=%wide.region_6.7_spmd.clone, body=%wide.region_1.6_spmd.clone.sunk | while | flops 286005248 | bytes 16725373 | solution.py:127
  146.2 6.3 %conditional.3 = ((f32[4,512]{1,0:T(4,128)S(1)}, f32[4,512]{1,0:T(4,128)S(1)}, f32[4,512,64]{1,2,0:T(8,128)S(1)})) conditional(s32[]{:T(128)} %convert_element_type.82, (f32[4,512]{1,0:T(4,128)S(1)}, f32[4,512]{1,0:T(4,128)S(1)}, f32[4,512,64]{1,2,0:T(8,128)S(1)}) %tuple.89, (s32[]{:T(128)}, s32[]{:T(128)}, bf16[4096,256]{0,1:T(8,128)(2,1)}, ...), branch_computations={%region_2.0_spmd, %region_3.5_spmd} | conditional | flops 286005248 | bytes 16723030 | solution.py:124
  147.2 1.1 constant_dynamic-slice_fusion
  148.2 1.2 fusion.4
  149.4 1.4 fusion.3
  150.8 1.6 fusion.8
  153.0 2.0 fusion.57
  155.1 2.8 %add_convert_fusion = bf16[512,2048]{1,0:T(8,128)(2,1)} fusion(f32[512,2048]{1,0:T(8,128)S(1)} %fusion.57, bf16[512,2048]{1,0:T(8,128)(2,1)S(1)} %copy-done, f32[512,512]{1,0:T(8,128)S(1)} %copy-done.3, f32[512]{0:T(512)S(1)} %copy-done.10, f32[512]{0:T(512)S(1)} %add_rsqrt_fusion), kind=kOutput, calls=%fused_computation.23 | convolution fusion | flops 1077673984 | bytes 9441280 | tf_op jit(solution)/shard_map/dot_general | solution.py:154
  158.5 73.3 %reduce-scatter.2.cloned.1.call-done = bf16[128,2048]{1,0:T(8,128)(2,1)} async-done(((bf16[512,2048]{1,0:T(8,128)(2,1)}), bf16[128,2048]{1,0:T(8,128)(2,1)}) %reduce-scatter.2.cloned.1.call-update) | async-done | bytes 524304 | tf_op jit(solution)/shard_map/reduce_scatter | solution.py:155
  (64 shorter events, 5.0 us)
Async XLA Ops:
  7.2 147.9 %copy-start = (bf16[512,2048]{1,0:T(8,128)(2,1)S(1)}, bf16[512,2048]{1,0:T(8,128)(2,1)}, u32[]{:S(2)}) copy-start(bf16[512,2048]{1,0:T(8,128)(2,1)} %param.27) | copy-start | bytes 6291460
  7.2 84.9 %all-gather.3.cloned.1.call-start = ((), (), s32[]{:S(2)}) async-start(), calls=%async_computation.2 | async-start | bytes 2359296 | tf_op jit(solution)/shard_map/all_gather | solution.py:105
  38.4 0.7 copy-start.5
  39.1 1.9 copy-start.7
  39.6 1.3 copy-start.1
  41.0 1.5 copy-start.8
  42.4 3.9 %copy-start.4 = (f32[31,512]{1,0:T(8,128)S(1)}, f32[31,512]{1,0:T(8,128)}, u32[]{:S(2)}) copy-start(f32[31,512]{1,0:T(8,128)} %param.23) | copy-start | bytes 190468
  42.4 99.5 %all-gather.5.cloned.1.call-start = ((), (), s32[]{:S(2)}) async-start(), calls=%async_computation.3 | async-start | bytes 2359296 | tf_op jit(solution)/shard_map/all_gather | solution.py:106
  45.5 186.4 %reduce-scatter.2.cloned.1.call-start = ((), (), s32[]{:S(2)}) async-start(), calls=%async_computation.4 | async-start | bytes 2621440 | tf_op jit(solution)/shard_map/reduce_scatter | solution.py:155
  46.3 3.8 %copy-start.2 = (bf16[512,2048]{1,0:T(8,128)(2,1)S(1)}, bf16[512,2048]{1,0:T(8,128)(2,1)}, u32[]{:S(2)}) copy-start(bf16[512,2048]{1,0:T(8,128)(2,1)} %copy-done.1) | copy-start | bytes 6291460
  46.3 3.8 %copy-start.6 = (bf16[2048,512]{1,0:T(8,128)(2,1)S(1)}, bf16[2048,512]{1,0:T(8,128)(2,1)}, u32[]{:S(2)}) copy-start(bf16[2048,512]{1,0:T(8,128)(2,1)} %param.21) | copy-start | bytes 6291460
  50.1 4.7 %copy-start.9 = (bf16[2048,256]{1,0:T(8,128)(2,1)S(1)}, bf16[2048,256]{1,0:T(8,128)(2,1)}, u32[]{:S(2)}) copy-start(bf16[2048,256]{1,0:T(8,128)(2,1)} %param.18) | copy-start | bytes 3145732
  51.4 5.0 %collective-permute-start = (bf16[30,512]{1,0:T(8,128)(2,1)S(1)}, bf16[30,512]{1,0:T(8,128)(2,1)S(1)}, u32[]{:S(2)}, u32[]{:S(2)}) collective-permute-start(bf16[30,512]{1,0:T(8,128)(2,1)S(1)} %slice.252), channel_id=1, source_target_pairs={{0,4},{4,8},{8,12},{12,16},{16,20},{20,24},{24,28},{1,5},{5,9},{9,... | collective-permute-start | bytes 92168 | tf_op jit(solution)/shard_map/ppermute | solution.py:12
  153.0 2.1 copy-start.3
  153.0 2.1 copy-start.10
Sparse Core Ops, SparseCore 0:
  42.5 49.5 all-gather.2
  94.3 47.6 all-gather.4
  158.1 73.7 reduce-scatter.1
